TPU v7x, 32 devices: a whole 2x2x4 slice. The times are simulated.
32 devices in a mesh: ep: 8 (over z, core), tp: 4 (over y, x).
Axes of the slice: x: 2, y: 2, z: 4, core: 2. Of those that a mesh axis runs over, the one named last changes fastest.
Arguments:
- first_batch_queries: bfloat16 [2048, 1024], P('ep', 'tp'), may hold values from -6 to 6
- first_batch_keys: bfloat16 [2048, 1024], P('ep', 'tp'), may hold values from -6 to 6
- first_batch_values: bfloat16 [2048, 2048], P('ep', 'tp'), may hold values from -6 to 6
- output_gate_preactivation: bfloat16 [2048, 2048], P('ep', 'tp'), may hold values from -6 to 6
- decay_preactivation: bfloat16 [2048, 1024], P('ep', 'tp'), may hold values from -6 to 6
- channel_decay_bias: float32 [1024], P('tp')
- added_log_decay: float32 [16, 2048], P('tp', 'ep'), may hold values from -0.7 to 0
- head_norm_gain: float32 [2048], P('tp'), may hold values from 0.1 to 1.9
- attention_output_weight: bfloat16 [2048, 2048], P(None, 'tp'), may hold values from -0.125 to 0.125
- second_batch_rows: bfloat16 [768, 2048], P('ep'), may hold values from -6 to 6
- expert_norm_gain: float32 [2048], replicated, may hold values from 0.1 to 1.9
- routed_expert_index: int32 [768, 4], P('ep'), may hold values from 0 to 7, all different within a row; in each aligned block of 96 rows (0 to 95, 96 to 191, ...) at most 72 rows name the same one
- router_chosen_scores: float32 [768, 4], P('ep'), may hold values from 0.1 to 1
- expert_gate_weight: bfloat16 [8, 2048, 4096], P('ep', None, 'tp'), may hold values from -0.125 to 0.125
- expert_up_weight: bfloat16 [8, 2048, 4096], P('ep', None, 'tp'), may hold values from -0.125 to 0.125
- expert_down_weight: bfloat16 [8, 4096, 2048], P('ep', None, 'tp'), may hold values from -0.09375 to 0.09375
- shared_gate_weight: bfloat16 [2048, 1024], P(None, 'tp'), may hold values from -0.125 to 0.125
- shared_up_weight: bfloat16 [2048, 1024], P(None, 'tp'), may hold values from -0.125 to 0.125
- shared_down_weight: bfloat16 [1024, 2048], P(None, 'tp'), may hold values from -0.1875 to 0.1875
Outputs:
- token_mixed: bfloat16 [2048, 2048], P('ep', 'tp')
- channel_mixed: bfloat16 [768, 2048], P('ep', 'tp')
Inputs may be any that keep to these rules, and one draw needn't show every extreme that they name: `routed_expert_index`: in each aligned block of 96 rows (the rows of one index of ep) no expert is named by more than 72 rows, a bound that some block reaches; a row names 4 different experts.
All inputs are finite; a program needn't handle non-finite values.
Results may differ from a plain program's by a relative error of at most 0.018.
Values may be sent and summed in bfloat16 or wider, within the bound.
A program may use at most 64 MiB of HBM per device.

v0:
```python
import jax
import jax.numpy as jnp
from jax import lax
from jax.sharding import PartitionSpec as P

BLOCK = 64
epsilon = 1e-06
temper = 16.0
routed_scale = 2.5
largest_value = lax.Precision.HIGHEST


def entering(value, axis, combine, identity):
    size, here = (lax.axis_size(axis), lax.axis_index(axis))
    everything = jax.tree.map(
        lambda part, kind: lax.all_gather(part.astype(kind), axis),
        value,
        (jnp.bfloat16, jnp.bfloat16),
    )
    start = jax.tree.map(
        lambda part, zero: jnp.broadcast_to(jnp.asarray(zero, part.dtype), part.shape),
        value,
        identity,
    )

    def hop(k, before):
        reached = k < here
        new = combine(
            before, jax.tree.map(lambda part, own: part[k].astype(own.dtype), everything, value)
        )
        return jax.tree.map(lambda a, b: jnp.where(reached, a, b), new, before)

    return lax.fori_loop(0, size, hop, start)


def head_norm(tensor, gain_rows):
    mean_square = jnp.mean(tensor * tensor, axis=-1, keepdims=True)
    return tensor * lax.rsqrt(mean_square + epsilon) * gain_rows


def log_decay_values(decay_preactivation, channel_decay_bias, added_log_decay):
    number_of_heads = added_log_decay.shape[0]
    row_count = decay_preactivation.shape[0]
    logits = decay_preactivation.astype(jnp.float32) + channel_decay_bias[None, :]
    baseline_log_decay = (jax.nn.log_sigmoid(logits) / temper).reshape(
        row_count, number_of_heads, -1
    )
    return baseline_log_decay + jnp.transpose(added_log_decay)[:, :, None]


def combine_states(earlier, latter):
    return (earlier[0] * latter[0], latter[0][..., None] * earlier[1] + latter[1])


def mixer_heads(
    first_batch_queries,
    first_batch_keys,
    first_batch_values,
    output_gate_preactivation,
    decay_preactivation,
    channel_decay_bias,
    added_log_decay,
    head_norm_gain,
):
    number_of_heads = added_log_decay.shape[0]
    row_count = first_batch_queries.shape[0]
    key_channel_width = first_batch_queries.shape[1] // number_of_heads
    value_width = first_batch_values.shape[1] // number_of_heads
    block_count = row_count // BLOCK

    def split_into_blocks(tensor, width):
        shaped = tensor.astype(jnp.float32).reshape(block_count, BLOCK, number_of_heads, width)
        return shaped.transpose(0, 2, 1, 3)

    queries = split_into_blocks(first_batch_queries, key_channel_width)
    keys_all = split_into_blocks(first_batch_keys, key_channel_width)
    values = split_into_blocks(first_batch_values, value_width)
    decay_factors = split_into_blocks(
        log_decay_values(decay_preactivation, channel_decay_bias, added_log_decay),
        key_channel_width,
    )
    running_state = jnp.cumsum(decay_factors, axis=2)
    block_number_total = running_state[:, :, -1, :]
    query_decayed = queries * jnp.exp(running_state)
    key_raised = keys_all * jnp.exp(-running_state)
    lower_mask = jnp.tril(jnp.ones((BLOCK, BLOCK), bool))
    attention_scores = jnp.einsum(
        "nhqd,nhkd->nhqk", query_decayed, key_raised, precision=largest_value
    )
    attention_scores = jnp.where(lower_mask, attention_scores, 0.0)
    within_block = jnp.einsum("nhqk,nhkv->nhqv", attention_scores, values, precision=largest_value)
    updates = jnp.einsum(
        "nhkd,nhkv->nhdv",
        keys_all * jnp.exp(block_number_total[:, :, None, :] - running_state),
        values,
        precision=largest_value,
    )

    def carry_blocks(carry_state, inputs):
        state_update, total_log = inputs
        return (jnp.exp(total_log)[..., None] * carry_state + state_update, carry_state)

    zero_state = jnp.zeros((number_of_heads, key_channel_width, value_width), jnp.float32)
    device_state, before = lax.scan(carry_blocks, zero_state, (updates, block_number_total))
    device_decay = jnp.exp(jnp.sum(block_number_total, axis=0))
    identity = (jnp.ones((number_of_heads, key_channel_width), jnp.float32), zero_state)
    _, incoming = entering((device_decay, device_state), "ep", combine_states, identity)
    lead_in = jnp.exp(jnp.cumsum(block_number_total, axis=0) - block_number_total)
    states = before + lead_in[..., None] * incoming[None]
    carried = jnp.einsum("nhqd,nhdv->nhqv", query_decayed, states, precision=largest_value)
    head_values = (
        (within_block + carried)
        .transpose(0, 2, 1, 3)
        .reshape(row_count, number_of_heads, value_width)
    )
    gate_rows = jax.nn.silu(output_gate_preactivation.astype(jnp.float32)).reshape(
        row_count, number_of_heads, value_width
    )
    gated_heads = (
        head_norm(head_values, head_norm_gain.reshape(number_of_heads, value_width)) * gate_rows
    )
    return gated_heads.reshape(row_count, number_of_heads * value_width).astype(jnp.bfloat16)


def expert_slots(route_rows, experts, capacity):
    flat_ids = route_rows.reshape(-1)
    targets = jnp.arange(experts, dtype=jnp.int32)
    onehot = (flat_ids[:, None] == targets[None, :]).astype(jnp.int32)
    earlier = jnp.cumsum(onehot, axis=0) - onehot
    return flat_ids * capacity + jnp.sum(earlier * onehot, axis=1)


def slot_owner(slot_ids, slot_count, top_count):
    matches = slot_ids[None, :] == jnp.arange(slot_count, dtype=jnp.int32)[:, None]
    token_ids = jnp.arange(slot_ids.shape[0], dtype=jnp.int32) // top_count
    return jnp.sum(jnp.where(matches, token_ids[None, :] + 1, 0), axis=1) - 1


def fill_slots(source_rows, owners):
    picked_rows = jnp.take(source_rows, jnp.maximum(owners, 0), axis=0)
    return jnp.where((owners >= 0)[:, None], picked_rows, jnp.zeros((), jnp.bfloat16))


def paired_rows(tensor, factor):
    return tensor.reshape(tensor.shape[0] // factor, tensor.shape[1] * factor)


def paired_product(section, weight, factor, own_width):
    row_count = section.shape[0]
    pieces = section.reshape(row_count, -1, factor, own_width)
    products = [
        jnp.dot(
            pieces[:, :, which, :].reshape(row_count, -1),
            weight,
            preferred_element_type=jnp.float32,
        )
        for which in range(factor)
    ]
    return jnp.stack(products, axis=1)


def local(
    first_batch_queries,
    first_batch_keys,
    first_batch_values,
    output_gate_preactivation,
    decay_preactivation,
    channel_decay_bias,
    added_log_decay,
    head_norm_gain,
    attention_output_weight,
    second_batch_rows,
    expert_norm_gain,
    routed_expert_index,
    router_chosen_scores,
    expert_gate_weight,
    expert_up_weight,
    expert_down_weight,
    shared_gate_weight,
    shared_up_weight,
    shared_down_weight,
):
    mixed_heads = mixer_heads(
        first_batch_queries,
        first_batch_keys,
        first_batch_values,
        output_gate_preactivation,
        decay_preactivation,
        channel_decay_bias,
        added_log_decay,
        head_norm_gain,
    )
    experts = lax.axis_size("ep")
    tokens, top_count = routed_expert_index.shape
    capacity = tokens * top_count * 3 // (2 * experts)
    slot_count = experts * capacity
    model_width = second_batch_rows.shape[1]
    features = second_batch_rows.astype(jnp.float32)
    normed = features * lax.rsqrt(jnp.mean(features * features, axis=1, keepdims=True) + epsilon)
    normed = (normed * expert_norm_gain[None, :]).astype(jnp.bfloat16)
    slot_ids = expert_slots(routed_expert_index, experts, capacity)
    owners = slot_owner(slot_ids, slot_count, top_count)
    gate_weight = expert_gate_weight[0]
    up_weight = expert_up_weight[0]
    down_weight = expert_down_weight[0]
    columns = model_width // lax.axis_size("tp")
    own_columns = lax.dynamic_slice_in_dim(normed, lax.axis_index("tp") * columns, columns, 1)
    outgoing = fill_slots(own_columns, owners).reshape(experts, capacity, columns)
    arrived = lax.all_to_all(outgoing, "ep", split_axis=0, concat_axis=0, tiled=True)
    flat_columns = arrived.reshape(slot_count, columns)
    section = lax.all_gather(flat_columns, "tp", axis=1, tiled=True)
    gate_value = jnp.dot(section, gate_weight, preferred_element_type=jnp.float32)
    up_value = jnp.dot(section, up_weight, preferred_element_type=jnp.float32)
    routed_hidden = (jax.nn.silu(gate_value) * up_value).astype(jnp.bfloat16)
    hidden_width = routed_hidden.shape[1]
    shared_gate_value = jnp.dot(normed, shared_gate_weight, preferred_element_type=jnp.float32)
    shared_up_value = jnp.dot(normed, shared_up_weight, preferred_element_type=jnp.float32)
    shared_hidden = (jax.nn.silu(shared_gate_value) * shared_up_value).astype(jnp.bfloat16)
    shared_width = shared_hidden.shape[1]
    shared_factor = hidden_width // shared_width
    shared_paired = paired_rows(shared_hidden, shared_factor)
    mixer_total = jnp.dot(
        lax.all_gather(mixed_heads, "tp", axis=1, tiled=True),
        attention_output_weight,
        preferred_element_type=jnp.float32,
    )
    routed_section = lax.all_gather(routed_hidden, "tp", axis=1, tiled=True)
    shared_section = lax.all_gather(shared_paired, "tp", axis=1, tiled=True)
    routed_part = jnp.dot(routed_section, down_weight, preferred_element_type=jnp.float32)
    shared_part = paired_product(shared_section, shared_down_weight, shared_factor, shared_width)
    shared_total = shared_part.reshape(tokens, -1)
    token_mixed = mixer_total.astype(jnp.bfloat16)
    routed_output = routed_part.astype(jnp.bfloat16).reshape(experts, capacity, -1)
    returned = lax.all_to_all(routed_output, "ep", split_axis=0, concat_axis=0, tiled=True).reshape(
        slot_count, -1
    )
    picked = jnp.take(returned, slot_ids, axis=0).astype(jnp.float32).reshape(tokens, top_count, -1)
    weights = (
        routed_scale * router_chosen_scores / jnp.sum(router_chosen_scores, axis=1, keepdims=True)
    )
    channel_mixed = (jnp.sum(weights[:, :, None] * picked, axis=1) + shared_total).astype(
        jnp.bfloat16
    )
    return (token_mixed, channel_mixed)


def solution(mesh):
    placed = (
        P("ep", "tp"),
        P("ep", "tp"),
        P("ep", "tp"),
        P("ep", "tp"),
        P("ep", "tp"),
        P("tp"),
        P("tp", "ep"),
        P("tp"),
        P(None, "tp"),
        P("ep", None),
        P(),
        P("ep", None),
        P("ep", None),
        P("ep", None, "tp"),
        P("ep", None, "tp"),
        P("ep", None, "tp"),
        P(None, "tp"),
        P(None, "tp"),
        P(None, "tp"),
    )
    return jax.shard_map(
        local, mesh=mesh, in_specs=placed, out_specs=(P("ep", "tp"), P("ep", "tp")), check_vma=False
    )
```

profile of v0, /device:TPU:0, one launch (start us, length us, event | category | flops | bytes accessed | tf_op | source)
XLA Modules:
  0.0 203.9 jit_solution(17407363473838470241)
XLA Ops:
  10.4 1.2 fusion.15
  11.8 1.2 fusion.17
  13.7 2.7 %gather_fusion = bf16[576,512]{1,0:T(8,128)(2,1)S(1)} fusion(bf16[96,512]{1,0:T(8,128)(2,1)S(1)} %constant_dynamic-slice_fusion, s32[1024]{0:T(1024)S(1)} %pad_clamp_fusion.1), kind=kCustom, calls=%fused_computation | custom fusion | bytes 1181952 | tf_op jit(solution)/shard_map/jit(_take)/gather | solution.py:140
  16.7 23.0 %all_to_all.10 = bf16[8,72,512]{2,1,0:T(8,128)(2,1)} all-to-all(bf16[8,72,512]{2,1,0:T(8,128)(2,1)S(1)} %select_select_fusion), channel_id=1, replica_groups=mesh['ep'=8,'tp'=4] {'ep'}, dimensions={0} | all-to-all | bytes 1179648 | tf_op jit(solution)/shard_map/all_to_all | solution.py:209
  40.6 1.7 reshape.254
  43.4 1.5 reduce_window_sum.37
  44.9 2.4 %fusion.23 = f32[4,4,64,128]{3,2,1,0:T(8,128)} fusion(f32[4,4,64,64]{3,2,1,0:T(8,128)S(1)} %reduce_window_sum.37, f32[4,64,4,64]{3,2,1,0:T(4,128)S(1)} %reshape.267, f32[4,4,64]{2,1,0:T(4,128)S(1)} %bitcast.133, bf16[4,64,4,128]{3,2,1,0:T(4,128)(2,1)} %reshape.254), kind=kOutput, calls=%fused_computation.48 | convolution fusion | flops 100794368 | bytes 1314816 | tf_op jit(solution)/shard_map/nhkd,nhkv->nhdv/dot_general | solution.py:92
  47.3 28.8 %all-gather.9.cloned.1.call-done = bf16[576,2048]{1,0:T(8,128)(2,1)} async-done(((bf16[576,512]{1,0:T(8,128)(2,1)}), bf16[576,2048]{1,0:T(8,128)(2,1)}) %all-gather.9.cloned.1.call-update) | async-done | bytes 2359312 | tf_op jit(solution)/shard_map/all_gather | solution.py:211
  76.1 5.2 %fusion.5 = f32[576,1024]{1,0:T(8,128)S(1)} fusion(bf16[576,2048]{1,0:T(8,128)(2,1)} %all-gather.9.cloned.1.call-done, bf16[1,2048,1024]{2,1,0:T(8,128)(2,1)} %param.36), kind=kOutput, calls=%fused_computation.12 | convolution fusion | flops 2415919104 | bytes 8912896 | tf_op jit(solution)/shard_map/dot_general | solution.py:212
  81.3 3.9 %multiply_convert_fusion = bf16[576,1024]{1,0:T(8,128)(2,1)} fusion(f32[576,1024]{1,0:T(8,128)S(1)} %fusion.5, bf16[576,2048]{1,0:T(8,128)(2,1)S(1)} %copy-done.20, bf16[1,2048,1024]{2,1,0:T(8,128)(2,1)S(1)} %copy-done.19), kind=kOutput, calls=%fused_computation.14 | convolution fusion | flops 2419458048 | bytes 10092544 | tf_op jit(solution)/shard_map/dot_general | solution.py:213
  85.3 6.9 %while.27 = (s32[]{:T(128)}, f32[4,64,128]{2,1,0:T(8,128)S(1)}, f32[4,4,64,128]{3,2,1,0:T(8,128)}, f32[4,4,64]{2,1,0:T(4,128)S(1)}, f32[4,4,64,128]{3,2,1,0:T(8,128)}, /*index=5*/s32[]{:T(128)}, s32[]{:T(128)}) while((s32[]{:T(128)}, f32[4,64,128]{2,1,0:T(8,128)S(1)}, f32[4,4,64,128]{3,2,1,0:T(8,128)}, f32[4,4,64]{2,1,0:T(4,128)S(1)}, ...), condition=%wide.region_2.3_spmd.clone, body=%wide.region_1.2_spmd.clone.sunk | while | flops 131075 | bytes 659040 | solution.py:104
  92.8 2.0 reshape.266
  94.8 12.5 %all-gather.2 = bf16[8,4,64]{2,1,0:T(4,128)(2,1)} all-gather(bf16[1,4,64]{2,1,0:T(4,128)(2,1)S(1)} %fusion.52), channel_id=2, replica_groups=mesh['ep'=8,'tp'=4] {'ep'}, dimensions={0}, use_global_device_ids=true | all-gather | bytes 4608 | tf_op jit(solution)/shard_map/all_gather | solution.py:16
  107.3 16.2 %all-gather.1 = bf16[32,64,128]{2,1,0:T(8,128)(2,1)} all-gather(bf16[4,64,128]{2,1,0:T(8,128)(2,1)} %convert_element_type.87), channel_id=3, replica_groups=mesh['ep'=8,'tp'=4] {'ep'}, dimensions={0}, use_global_device_ids=true | all-gather | bytes 589824 | tf_op jit(solution)/shard_map/all_gather | solution.py:16
  123.6 2.1 %convolution_select_fusion = f32[4,4,64,64]{3,2,1,0:T(8,128)S(1)} fusion(f32[4,4,64,64]{3,2,1,0:T(8,128)S(1)} %reduce_window_sum.37, f32[4,64,4,64]{3,2,1,0:T(4,128)S(1)} %reshape.267, f32[4,64,4,64]{3,2,1,0:T(4,128)} %reshape.266, pred[64,64]{1,0:T(8,128)(4,1)S(1)} %iota_compare_fusion.1), kind=kOutput, calls=%fused_computation.16 | convolution fusion | flops 50593792 | bytes 1052672 | tf_op jit(solution)/shard_map/nhqd,nhkd->nhqk/dot_general | solution.py:87
  125.7 1.2 fusion.37
  126.9 13.2 %while.28 = (s32[]{:T(128)}, f32[4,64,128]{2,1,0:T(8,128)S(1)}, s32[]{:T(128)}, bf16[8,4,64]{2,1,0:T(4,128)(2,1)}, bf16[8,4,64,128]{3,2,1,0:T(8,128)(2,1)}, /*index=5*/s32[]{:T(128)}, s32[]{:T(128)}) while((s32[]{:T(128)}, f32[4,64,128]{2,1,0:T(8,128)S(1)}, s32[]{:T(128)}, bf16[8,4,64]{2,1,0:T(4,128)(2,1)}, ...), condition=%wide.region_6.7_spmd.clone, body=%wide.region_5.6_spmd.clone.sunk | while | flops 164100 | bytes 330345 | solution.py:33
  140.1 2.8 %multiply_reduce_fusion.1 = (f32[4,64,4]{1,2,0:T(4,128)S(1)}, f32[4,64,4,128]{3,1,2,0:T(8,128)}) fusion(f32[4,4,64,128]{3,2,1,0:T(8,128)} %fusion.37, f32[4,4,64,128]{3,2,1,0:T(8,128)} %get-tuple-element.124, f32[4,64,128]{2,1,0:T(8,128)S(1)} %get-tuple-element.126, f32[4,4,64]{2,1,0:T(4,128)S(1)} %fusion.14, f32[4,64,4,64]{3,2,1,0:T(4,128)S(1)} %copy-done.2, ...), kind=kOutput, calls=%fused_computation.52 | convolution fusion | flops 101383168 | bytes 2236416 | tf_op jit(solution)/shard_map/nhqd,nhdv->nhqv/dot_general | solution.py:110
  143.1 1.4 copy.97
  144.8 1.6 fusion.31
  150.1 1.6 fusion.53
  151.6 2.2 %fusion.13 = bf16[96,256]{1,0:T(8,128)(2,1)} fusion(bf16[96,2048]{1,0:T(8,128)(2,1)S(1)} %copy-done.4, bf16[2048,256]{1,0:T(8,128)(2,1)} %param.40, f32[96,256]{1,0:T(8,128)S(1)} %fusion.53), kind=kOutput, calls=%fused_computation.21 | convolution fusion | flops 100810752 | bytes 1589248 | tf_op jit(solution)/shard_map/dot_general | solution.py:217
  154.6 8.7 %all_gather.28 = bf16[24,4096]{1,0:T(8,128)(2,1)S(1)} all-gather(bf16[24,1024]{1,0:T(8,128)(2,1)S(1)} %reshape.261), channel_id=1, replica_groups=mesh['ep'=8,'tp'=4] {'tp'}, dimensions={1}, use_global_device_ids=true | all-gather | bytes 245760 | tf_op jit(solution)/shard_map/all_gather | solution.py:228
  163.5 1.5 slice_reduce_fusion.3
  166.5 7.1 %fusion.9 = bf16[576,512]{1,0:T(8,128)(2,1)} fusion(bf16[576,4096]{1,0:T(8,128)(2,1)} %all-gather.11.cloned.1.call-done, bf16[1,4096,512]{2,1,0:T(8,128)(2,1)} %param.38), kind=kOutput, calls=%fused_computation.15 | convolution fusion | flops 2416214016 | bytes 9502720 | tf_op jit(solution)/shard_map/dot_general | solution.py:229
  173.6 3.7 %all-to-all-start.1 = ((bf16[8,72,512]{2,1,0:T(8,128)(2,1)}), bf16[8,72,512]{2,1,0:T(8,128)(2,1)S(1)}, u32[]{:S(2)}, u32[]{:S(2)}) async-start(bf16[8,72,512]{2,1,0:T(8,128)(2,1)} %bitcast.17), calls=%async_computation.1 | async-start | bytes 1179648 | tf_op jit(solution)/shard_map/all_to_all | solution.py:234
  177.3 1.5 convolution_bitcast_fusion.1
  179.3 1.5 convolution_bitcast_fusion.2
  180.7 1.5 convolution_bitcast_fusion.3
  182.5 2.6 %convolution_convert_fusion = bf16[256,512]{1,0:T(8,128)(2,1)} fusion(bf16[256,2048]{1,0:T(8,128)(2,1)} %all-gather.7.cloned.1.call-done, bf16[2048,512]{1,0:T(8,128)(2,1)S(1)} %copy-done), kind=kOutput, calls=%fused_computation.19 | convolution fusion | flops 537001984 | bytes 3407872 | tf_op jit(solution)/shard_map/dot_general | solution.py:222
  185.2 8.7 %all-to-all-done.1 = bf16[8,72,512]{2,1,0:T(8,128)(2,1)S(1)} async-done(((bf16[8,72,512]{2,1,0:T(8,128)(2,1)}), bf16[8,72,512]{2,1,0:T(8,128)(2,1)S(1)}, u32[]{:S(2)}, u32[]{:S(2)}) %all-to-all-start.1) | async-done | bytes 589856 | tf_op jit(solution)/shard_map/all_to_all | solution.py:234
  193.9 2.1 %gather_fusion.1 = bf16[384,512]{1,0:T(8,128)(2,1)S(1)} fusion(bf16[576,512]{1,0:T(8,128)(2,1)S(1)} %bitcast.126, s32[1024]{0:T(1024)S(1)} %pad_clamp_fusion), kind=kCustom, calls=%fused_computation.1 | custom fusion | bytes 787968 | tf_op jit(solution)/shard_map/jit(_take)/gather | solution.py:237
  (138 shorter events, 35.5 us)
Async XLA Ops:
  7.2 175.4 %copy-start = (bf16[2048,512]{1,0:T(8,128)(2,1)S(1)}, bf16[2048,512]{1,0:T(8,128)(2,1)}, u32[]{:S(2)}) copy-start(bf16[2048,512]{1,0:T(8,128)(2,1)} %param.31) | copy-start | bytes 6291460
  7.2 68.9 %all-gather.9.cloned.1.call-start = ((), (), s32[]{:S(2)}) async-start(), calls=%async_computation.3 | async-start | bytes 2949120 | tf_op jit(solution)/shard_map/all_gather | solution.py:211
  9.6 0.6 copy-start.13
  12.9 0.8 copy-start.3
  16.5 23.4 %copy-start.11 = (bf16[256,256]{1,0:T(8,128)(2,1)S(1)}, bf16[256,256]{1,0:T(8,128)(2,1)}, u32[]{:S(2)}) copy-start(bf16[256,256]{1,0:T(8,128)(2,1)} %param.27) | copy-start | bytes 393220
  16.5 23.4 %copy-start.18 = (f32[256]{0:T(256)S(1)}, f32[256]{0:T(256)}, u32[]{:S(2)}) copy-start(f32[256]{0:T(256)} %param.28) | copy-start | bytes 3076
  16.5 23.8 %copy-start.16 = (f32[4,256]{1,0:T(4,128)S(1)}, f32[4,256]{1,0:T(4,128)}, u32[]{:S(2)}) copy-start(f32[4,256]{1,0:T(4,128)} %param.29) | copy-start | bytes 12292
  16.5 23.9 %copy-start.12 = (bf16[256,256]{1,0:T(8,128)(2,1)S(1)}, bf16[256,256]{1,0:T(8,128)(2,1)}, u32[]{:S(2)}) copy-start(bf16[256,256]{1,0:T(8,128)(2,1)} %param.24) | copy-start | bytes 393220
  39.8 126.7 %all-gather.11.cloned.1.call-start = ((), (), s32[]{:S(2)}) async-start(), calls=%async_computation.4 | async-start | bytes 5898240 | tf_op jit(solution)/shard_map/all_gather | solution.py:227
  76.1 5.2 %copy-start.19 = (bf16[1,2048,1024]{2,1,0:T(8,128)(2,1)S(1)}, bf16[1,2048,1024]{2,1,0:T(8,128)(2,1)}, u32[]{:S(2)}) copy-start(bf16[1,2048,1024]{2,1,0:T(8,128)(2,1)} %param.37) | copy-start | bytes 12582916
  76.1 5.3 %copy-start.20 = (bf16[576,2048]{1,0:T(8,128)(2,1)S(1)}, bf16[576,2048]{1,0:T(8,128)(2,1)}, u32[]{:S(2)}) copy-start(bf16[576,2048]{1,0:T(8,128)(2,1)} %all-gather.9.cloned.1.call-done) | copy-start | bytes 7077892
  85.2 97.3 %all-gather.7.cloned.1.call-start = ((), (), s32[]{:S(2)}) async-start(), calls=%async_computation.2 | async-start | bytes 1310720 | tf_op jit(solution)/shard_map/all_gather | solution.py:223
  92.8 32.9 %copy-start.5 = (bf16[4,64,4,128]{3,2,1,0:T(4,128)(2,1)S(1)}, bf16[4,64,4,128]{3,2,1,0:T(4,128)(2,1)}, u32[]{:S(2)}) copy-start(bf16[4,64,4,128]{3,2,1,0:T(4,128)(2,1)} %reshape.254) | copy-start | bytes 786436
  125.7 14.4 %copy-start.2 = (f32[4,64,4,64]{3,2,1,0:T(4,128)S(1)}, f32[4,64,4,64]{3,2,1,0:T(4,128)}, u32[]{:S(2)}) copy-start(f32[4,64,4,64]{3,2,1,0:T(4,128)} %reshape.266) | copy-start | bytes 786436
  140.1 4.7 %copy-start.6 = (bf16[256,512]{1,0:T(8,128)(2,1)S(1)}, bf16[256,512]{1,0:T(8,128)(2,1)}, u32[]{:S(2)}) copy-start(bf16[256,512]{1,0:T(8,128)(2,1)} %param.26) | copy-start | bytes 786436
  142.9 3.5 %copy-start.15 = (s32[96,4]{0,1:T(4,128)S(1)}, s32[96,4]{0,1:T(4,128)}, u32[]{:S(2)}) copy-start(s32[96,4]{0,1:T(4,128)} %param.34) | copy-start | bytes 4612
  142.9 3.5 %copy-start.14 = (s32[384]{0:T(512)S(1)}, s32[384]{0:T(512)}, u32[]{:S(2)}) copy-start(s32[384]{0:T(512)} %copy-done.13) | copy-start | bytes 4612
  142.9 7.1 %copy-start.4 = (bf16[96,2048]{1,0:T(8,128)(2,1)S(1)}, bf16[96,2048]{1,0:T(8,128)(2,1)}, u32[]{:S(2)}) copy-start(bf16[96,2048]{1,0:T(8,128)(2,1)} %copy-done.3) | copy-start | bytes 1179652
  147.2 18.5 %copy-start.1 = (bf16[1024,512]{1,0:T(8,128)(2,1)S(1)}, bf16[1024,512]{1,0:T(8,128)(2,1)}, u32[]{:S(2)}) copy-start(bf16[1024,512]{1,0:T(8,128)(2,1)} %param.41) | copy-start | bytes 3145732
  166.5 10.8 %copy-start.8 = (bf16[3,8,4,256]{3,1,2,0:T(8,128)(2,1)S(1)}, bf16[3,8,4,256]{3,1,2,0:T(8,128)(2,1)}, u32[]{:S(2)}) copy-start(bf16[3,8,4,256]{3,1,2,0:T(8,128)(2,1)} %copy.114) | copy-start | bytes 147460
  173.6 5.4 %copy-start.17 = (pred[96,4]{0,1:T(4,128)(4,1)S(1)}, pred[96,4]{0,1:T(4,128)(4,1)}, u32[]{:S(2)}) copy-start(pred[96,4]{0,1:T(4,128)(4,1)} %compare_and_fusion) | copy-start | bytes 1156
  173.6 5.6 %copy-start.10 = (bf16[24,4,256]{2,1,0:T(4,128)(2,1)S(1)}, bf16[24,4,256]{2,1,0:T(4,128)(2,1)}, u32[]{:S(2)}) copy-start(bf16[24,4,256]{2,1,0:T(4,128)(2,1)} %get-tuple-element.166) | copy-start | bytes 147460
  173.6 5.7 %copy-start.9 = (bf16[24,4,256]{2,1,0:T(4,128)(2,1)S(1)}, bf16[24,4,256]{2,1,0:T(4,128)(2,1)}, u32[]{:S(2)}) copy-start(bf16[24,4,256]{2,1,0:T(4,128)(2,1)} %get-tuple-element.163) | copy-start | bytes 147460
  173.6 8.6 %copy-start.7 = (f32[24,1,512]{2,0,1:T(8,128)S(1)}, f32[24,1,512]{2,0,1:T(8,128)}, u32[]{:S(2)}) copy-start(f32[24,1,512]{2,0,1:T(8,128)} %convolution_bitcast_fusion) | copy-start | bytes 147460
  173.6 20.3 %all-to-all-start.1 = ((bf16[8,72,512]{2,1,0:T(8,128)(2,1)}), bf16[8,72,512]{2,1,0:T(8,128)(2,1)S(1)}, u32[]{:S(2)}, u32[]{:S(2)}) async-start(bf16[8,72,512]{2,1,0:T(8,128)(2,1)} %bitcast.17), calls=%async_computation.1 | async-start | bytes 1179648 | tf_op jit(solution)/shard_map/all_to_all | solution.py:234
Sparse Core Ops, SparseCore 0:
  39.9 36.1 all-gather.8
  85.4 56.9 all-gather.10
  146.5 25.0 all-gather.6
where the time goes:
time: 206 us; the launch traced here: 204 us
  blocking collectives  60.4 us (29%)
  waiting for transfers between devices  37.6 us (18%)
  matrix products  36.3 us (18%)
  other arithmetic  31.8 us (15%)
  local copies, waits for them, and re-layouts  19.5 us (9%)
  between operations  14.3 us (7%)
  starting transfers between devices  3.8 us (2%)
    all_gather x1, waiting for transfers between devices, local(): section = lax.all_gather(flat_columns, 'tp', axis=1, tiled=True)  28.8 us
    all_gather x2, blocking collectives, entering(): lax.all_gather(part.astype(kind), axis)  28.7 us
    all_to_all x1, blocking collectives, local(): lax.all_to_all(outgoing, 'ep', split_axis=0, concat_axis=0, tiled=True)  23 us
    all_to_all x1, waiting for transfers between devices, local(): lax.all_to_all(routed_output, 'ep', split_axis=0, concat_axis=0, tiled=True)  8.75 us
    all_gather x1, blocking collectives, local(): shared_section = lax.all_gather(shared_paired, 'tp', axis=1, tiled=True)  8.68 us
    select_n x8, other arithmetic, hop(): return jax.tree.map(lambda a, b: jnp.where(reached, a, b), new, before)  7.73 us
    dot_general x1, matrix products, local(): jnp.dot(routed_section, down_weight, preferred_element_type=jnp.float32)  7.07 us
    dot_general x4, matrix products, paired_product(): jnp.dot(pieces[:, :, which, :].reshape(row_count, -1), weight, preferred_...  5.29 us
  transfers between devices with their start and end apart: 4, of which 2 were waited for; matrix products, arithmetic and copies ran while one was open for 32% of the time, Pallas kernels for 0%

commit v1 on v0

--- a/solution.py
+++ b/solution.py
@@ -8,6 +8,29 @@
 temper = 16.0
 routed_scale = 2.5
 largest_value = lax.Precision.HIGHEST
+
+
+def cut_along(x, dim, length):
+    before, after = (x.shape[:dim], x.shape[dim + 1 :])
+    return jnp.moveaxis(x.reshape(*before, length, -1, *after), dim, 0)
+
+
+def laid_out(blocks, dim):
+    blocks = jnp.moveaxis(blocks, 0, dim)
+    lengths = blocks.shape
+    return blocks.reshape(*lengths[:dim], lengths[dim] * lengths[dim + 1], *lengths[dim + 2 :])
+
+
+def sent_to_each(value, axis, split_dim, concat_dim):
+    size, place = (lax.axis_size(axis), lax.axis_index(axis))
+    pieces = cut_along(value, split_dim, size)
+    out = pieces
+    for step in range(1, size):
+        target, source = ((place + step) % size, (place - step) % size)
+        sent = lax.dynamic_index_in_dim(pieces, target, 0)
+        received = lax.ppermute(sent, axis, [(i, (i + step) % size) for i in range(size)])
+        out = lax.dynamic_update_slice_in_dim(out, received, source, axis=0)
+    return laid_out(out, concat_dim)
 
 
 def entering(value, axis, combine, identity):
@@ -231,9 +254,7 @@
     shared_total = shared_part.reshape(tokens, -1)
     token_mixed = mixer_total.astype(jnp.bfloat16)
     routed_output = routed_part.astype(jnp.bfloat16).reshape(experts, capacity, -1)
-    returned = lax.all_to_all(routed_output, "ep", split_axis=0, concat_axis=0, tiled=True).reshape(
-        slot_count, -1
-    )
+    returned = sent_to_each(routed_output, "ep", 0, 0).reshape(slot_count, -1)
     picked = jnp.take(returned, slot_ids, axis=0).astype(jnp.float32).reshape(tokens, top_count, -1)
     weights = (
         routed_scale * router_chosen_scores / jnp.sum(router_chosen_scores, axis=1, keepdims=True)

time: 206 us -> 198 us (0.961)
  other arithmetic: 31.8 us -> 26.3 us
  matrix products: 36.3 us -> 31.3 us
  starting transfers between devices: 3.8 us -> 6.94 us
    all_to_all x1 -> x0, waiting for transfers between devices: 8.75 us -> none  [local(): lax.all_to_all(routed_output, 'ep', split_axis=0, concat_axis=0, tiled=True)]
    ppermute x0 -> x7, waiting for transfers between devices: none -> 8.4 us  [sent_to_each(): lax.ppermute(sent, axis, [(i, (i + step) % size) for i in range(size)])]
    ppermute x0 -> x7, starting transfers between devices: none -> 6.82 us  [sent_to_each(): lax.ppermute(sent, axis, [(i, (i + step) % size) for i in range(size)])]
    convert_element_type x8, other arithmetic: 5.27 us -> 0.06 us  [hop(): part[k].astype(own.dtype)]
    dot_general x4, matrix products: 5.29 us -> 0.98 us  [paired_product(): jnp.dot(pieces[:, :, which, :].reshape(row_count, -1), weight, preferred_...]
    all_to_all x1 -> x0, starting transfers between devices: 3.68 us -> none  [local(): lax.all_to_all(routed_output, 'ep', split_axis=0, concat_axis=0, tiled=True)]
  transfers between devices with their start and end apart: 4 -> 10, of which waited for: 2 -> 5; matrix products, arithmetic and copies ran while one was open for 32% -> 28% of each run, Pallas kernels for 0% -> 0%
where the time goes in v1:
time: 198 us; the launch traced here: 195 us
  blocking collectives  60.6 us (31%)
  waiting for transfers between devices  37.3 us (19%)
  matrix products  31.3 us (16%)
  other arithmetic  26.3 us (13%)
  local copies, waits for them, and re-layouts  17.7 us (9%)
  between operations  14.5 us (7%)
  starting transfers between devices  6.94 us (4%)
    all_gather x1, waiting for transfers between devices, local(): section = lax.all_gather(flat_columns, 'tp', axis=1, tiled=True)  28.8 us
    all_gather x2, blocking collectives, entering(): lax.all_gather(part.astype(kind), axis)  27.9 us
    all_to_all x1, blocking collectives, local(): lax.all_to_all(outgoing, 'ep', split_axis=0, concat_axis=0, tiled=True)  23 us
    all_gather x1, blocking collectives, local(): shared_section = lax.all_gather(shared_paired, 'tp', axis=1, tiled=True)  9.74 us
    ppermute x7, waiting for transfers between devices, sent_to_each(): lax.ppermute(sent, axis, [(i, (i + step) % size) for i in range(size)])  8.4 us
    select_n x8, other arithmetic, hop(): return jax.tree.map(lambda a, b: jnp.where(reached, a, b), new, before)  7.76 us
    ppermute x7, starting transfers between devices, sent_to_each(): lax.ppermute(sent, axis, [(i, (i + step) % size) for i in range(size)])  6.82 us
    dot_general x1, matrix products, local(): jnp.dot(routed_section, down_weight, preferred_element_type=jnp.float32)  6.39 us
  transfers between devices with their start and end apart: 10, of which 5 were waited for; matrix products, arithmetic and copies ran while one was open for 28% of the time, Pallas kernels for 0%

profile of v1, /device:TPU:0, one launch (start us, length us, event | category | flops | bytes accessed | tf_op | source)
XLA Modules:
  0.0 195.0 jit_solution(16255703731687574404)
XLA Ops:
  9.8 1.2 fusion.15
  11.2 1.2 fusion.17
  13.1 2.7 %gather_fusion = bf16[576,512]{1,0:T(8,128)(2,1)S(1)} fusion(bf16[96,512]{1,0:T(8,128)(2,1)S(1)} %constant_dynamic-slice_fusion.7, s32[1024]{0:T(1024)S(1)} %pad_clamp_fusion.1), kind=kCustom, calls=%fused_computation | custom fusion | bytes 1181952 | tf_op jit(solution)/shard_map/jit(_take)/gather | solution.py:163
  16.2 23.0 %all_to_all.5 = bf16[8,72,512]{2,1,0:T(8,128)(2,1)} all-to-all(bf16[8,72,512]{2,1,0:T(8,128)(2,1)S(1)} %select_select_fusion), channel_id=1, replica_groups=mesh['ep'=8,'tp'=4] {'ep'}, dimensions={0} | all-to-all | bytes 1179648 | tf_op jit(solution)/shard_map/all_to_all | solution.py:232
  40.1 1.7 reshape.248
  42.8 1.5 reduce_window_sum.37
  44.3 2.4 %fusion.23 = f32[4,4,64,128]{3,2,1,0:T(8,128)} fusion(f32[4,4,64,64]{3,2,1,0:T(8,128)S(1)} %reduce_window_sum.37, f32[4,64,4,64]{3,2,1,0:T(4,128)S(1)} %reshape.259, f32[4,4,64]{2,1,0:T(4,128)S(1)} %bitcast.135, bf16[4,64,4,128]{3,2,1,0:T(4,128)(2,1)} %reshape.248), kind=kOutput, calls=%fused_computation.48 | convolution fusion | flops 100794368 | bytes 1314816 | tf_op jit(solution)/shard_map/nhkd,nhkv->nhdv/dot_general | solution.py:115
  46.7 28.8 %all-gather.9.cloned.1.call-done = bf16[576,2048]{1,0:T(8,128)(2,1)} async-done(((bf16[576,512]{1,0:T(8,128)(2,1)}), bf16[576,2048]{1,0:T(8,128)(2,1)}) %all-gather.9.cloned.1.call-update) | async-done | bytes 2359312 | tf_op jit(solution)/shard_map/all_gather | solution.py:234
  75.5 5.2 %fusion.5 = f32[576,1024]{1,0:T(8,128)S(1)} fusion(bf16[576,2048]{1,0:T(8,128)(2,1)} %all-gather.9.cloned.1.call-done, bf16[1,2048,1024]{2,1,0:T(8,128)(2,1)} %param.36), kind=kOutput, calls=%fused_computation.12 | convolution fusion | flops 2415919104 | bytes 8912896 | tf_op jit(solution)/shard_map/dot_general | solution.py:235
  80.8 3.9 %multiply_convert_fusion = bf16[576,1024]{1,0:T(8,128)(2,1)} fusion(f32[576,1024]{1,0:T(8,128)S(1)} %fusion.5, bf16[576,2048]{1,0:T(8,128)(2,1)S(1)} %copy-done.14, bf16[1,2048,1024]{2,1,0:T(8,128)(2,1)S(1)} %copy-done.13), kind=kOutput, calls=%fused_computation.14 | convolution fusion | flops 2419458048 | bytes 10092544 | tf_op jit(solution)/shard_map/dot_general | solution.py:236
  84.7 6.9 %while.27 = (s32[]{:T(128)}, f32[4,64,128]{2,1,0:T(8,128)S(1)}, f32[4,4,64,128]{3,2,1,0:T(8,128)}, f32[4,4,64]{2,1,0:T(4,128)S(1)}, f32[4,4,64,128]{3,2,1,0:T(8,128)}, /*index=5*/s32[]{:T(128)}, s32[]{:T(128)}) while((s32[]{:T(128)}, f32[4,64,128]{2,1,0:T(8,128)S(1)}, f32[4,4,64,128]{3,2,1,0:T(8,128)}, f32[4,4,64]{2,1,0:T(4,128)S(1)}, ...), condition=%wide.region_2.3_spmd.clone, body=%wide.region_1.2_spmd.clone.sunk | while | flops 131075 | bytes 659040 | solution.py:127
  88.8 1.0 bitcast_add_fusion.2
  90.5 1.0 bitcast_add_fusion.2
  91.6 2.0 %reshape.258 = f32[4,64,4,64]{3,2,1,0:T(4,128)} reshape(bf16[256,256]{1,0:T(8,128)(2,1)} %param.23) | data formatting | bytes 393216 | tf_op jit(solution)/shard_map/transpose | solution.py:96
  93.6 11.8 %all-gather.2 = bf16[8,4,64]{2,1,0:T(4,128)(2,1)S(1)} all-gather(bf16[1,4,64]{2,1,0:T(4,128)(2,1)S(1)} %fusion.52), channel_id=2, replica_groups=mesh['ep'=8,'tp'=4] {'ep'}, dimensions={0}, use_global_device_ids=true | all-gather | bytes 4608 | tf_op jit(solution)/shard_map/all_gather | solution.py:39
  105.5 16.0 %all-gather.1 = bf16[32,64,128]{2,1,0:T(8,128)(2,1)} all-gather(bf16[4,64,128]{2,1,0:T(8,128)(2,1)S(1)} %convert_element_type.87), channel_id=3, replica_groups=mesh['ep'=8,'tp'=4] {'ep'}, dimensions={0}, use_global_device_ids=true | all-gather | bytes 589824 | tf_op jit(solution)/shard_map/all_gather | solution.py:39
  121.5 2.1 %convolution_select_fusion = f32[4,4,64,64]{3,2,1,0:T(8,128)S(1)} fusion(f32[4,4,64,64]{3,2,1,0:T(8,128)S(1)} %reduce_window_sum.37, f32[4,64,4,64]{3,2,1,0:T(4,128)S(1)} %reshape.259, f32[4,64,4,64]{3,2,1,0:T(4,128)} %reshape.258, pred[64,64]{1,0:T(8,128)(4,1)S(1)} %iota_compare_fusion.1), kind=kOutput, calls=%fused_computation.16 | convolution fusion | flops 50593792 | bytes 1052672 | tf_op jit(solution)/shard_map/nhqd,nhkd->nhqk/dot_general | solution.py:110
  123.7 1.2 fusion.37
  124.9 8.1 %while.28 = (s32[]{:T(128)}, f32[4,64,128]{2,1,0:T(8,128)S(1)}, s32[]{:T(128)}, bf16[8,4,64]{2,1,0:T(4,128)(2,1)S(1)}, bf16[8,4,64,128]{3,2,1,0:T(8,128)(2,1)}, /*index=5*/s32[]{:T(128)}, s32[]{:T(128)}) while((s32[]{:T(128)}, f32[4,64,128]{2,1,0:T(8,128)S(1)}, s32[]{:T(128)}, bf16[8,4,64]{2,1,0:T(4,128)(2,1)S(1)}, ...), condition=%wide.region_6.7_spmd.clone, body=%wide.region_5.6_spmd.clone.sunk | while | flops 164100 | bytes 330345 | solution.py:56
  133.0 2.8 %multiply_reduce_fusion.1 = (f32[4,64,4]{1,2,0:T(4,128)S(1)}, f32[4,64,4,128]{3,1,2,0:T(8,128)}) fusion(f32[4,4,64,128]{3,2,1,0:T(8,128)} %fusion.37, f32[4,4,64,128]{3,2,1,0:T(8,128)} %get-tuple-element.124, f32[4,64,128]{2,1,0:T(8,128)S(1)} %get-tuple-element.126, f32[4,4,64]{2,1,0:T(4,128)S(1)} %fusion.14, f32[4,64,4,64]{3,2,1,0:T(4,128)S(1)} %copy-done.2, ...), kind=kOutput, calls=%fused_computation.52 | convolution fusion | flops 101383168 | bytes 2236416 | tf_op jit(solution)/shard_map/nhqd,nhdv->nhqv/dot_general | solution.py:133
  135.9 1.4 copy.97
  137.6 1.8 fusion.31
  143.1 1.5 fusion.53
  144.7 2.2 %fusion.13 = bf16[96,256]{1,0:T(8,128)(2,1)} fusion(bf16[96,2048]{1,0:T(8,128)(2,1)S(1)} %copy-done.4, bf16[2048,256]{1,0:T(8,128)(2,1)} %param.40, f32[96,256]{1,0:T(8,128)S(1)} %fusion.53), kind=kOutput, calls=%fused_computation.21 | convolution fusion | flops 100810752 | bytes 1589248 | tf_op jit(solution)/shard_map/dot_general | solution.py:240
  147.7 9.7 %all_gather.28 = bf16[24,4096]{1,0:T(8,128)(2,1)S(1)} all-gather(bf16[24,1024]{1,0:T(8,128)(2,1)S(1)} %reshape.253), channel_id=1, replica_groups=mesh['ep'=8,'tp'=4] {'tp'}, dimensions={1}, use_global_device_ids=true | all-gather | bytes 245760 | tf_op jit(solution)/shard_map/all_gather | solution.py:251
  160.5 6.4 %fusion.9 = bf16[576,512]{1,0:T(8,128)(2,1)S(1)} fusion(bf16[576,4096]{1,0:T(8,128)(2,1)} %all-gather.11.cloned.1.call-done, bf16[1,4096,512]{2,1,0:T(8,128)(2,1)} %param.38), kind=kOutput, calls=%fused_computation.15 | convolution fusion | flops 2416214016 | bytes 9502720 | tf_op jit(solution)/shard_map/dot_general | solution.py:252
  167.0 5.5 %collective-permute-done = bf16[1,1,72,512]{3,2,0,1:T(8,128)(2,1)S(1)} collective-permute-done((bf16[1,1,72,512]{3,2,0,1:T(8,128)(2,1)S(1)}, bf16[1,1,72,512]{3,2,0,1:T(8,128)(2,1)S(1)}, u32[]{:S(2)}, u32[]{:S(2)}) %collective-permute-start) | collective-permute-done | bytes 73760 | tf_op jit(solution)/shard_map/ppermute | solution.py:31
  172.7 2.6 %convolution_convert_fusion = bf16[256,512]{1,0:T(8,128)(2,1)} fusion(bf16[256,2048]{1,0:T(8,128)(2,1)} %all-gather.7.cloned.1.call-done, bf16[2048,512]{1,0:T(8,128)(2,1)S(1)} %copy-done), kind=kOutput, calls=%fused_computation.19 | convolution fusion | flops 537001984 | bytes 3407872 | tf_op jit(solution)/shard_map/dot_general | solution.py:245
  176.4 1.6 collective-permute-start.4
  178.0 3.8 %collective-permute-start.5 = (bf16[1,1,72,512]{3,2,0,1:T(8,128)(2,1)S(1)}, bf16[1,1,72,512]{3,2,0,1:T(8,128)(2,1)S(1)}, u32[]{:S(2)}, u32[]{:S(2)}) collective-permute-start(bf16[1,1,72,512]{3,2,0,1:T(8,128)(2,1)S(1)} %get-tuple-element.188), channel_id=1, source_target_pairs={{0,24},{4,28},{8,0},{12,4},{16,8},{20,12},{24,16},{28,20},{1,25},{... | collective-permute-start | bytes 221192 | tf_op jit(solution)/shard_map/ppermute | solution.py:31
  182.6 1.6 collective-permute-done.3
  185.0 2.1 %gather_fusion.1 = bf16[384,512]{1,0:T(8,128)(2,1)S(1)} fusion(bf16[576,512]{1,0:T(8,128)(2,1)S(1)} %bitcast.128, s32[1024]{0:T(1024)S(1)} %pad_clamp_fusion), kind=kCustom, calls=%fused_computation.1 | custom fusion | bytes 787968 | tf_op jit(solution)/shard_map/jit(_take)/gather | solution.py:258
  (146 shorter events, 30.2 us)
Async XLA Ops:
  7.2 165.5 %copy-start = (bf16[2048,512]{1,0:T(8,128)(2,1)S(1)}, bf16[2048,512]{1,0:T(8,128)(2,1)}, u32[]{:S(2)}) copy-start(bf16[2048,512]{1,0:T(8,128)(2,1)} %param.31) | copy-start | bytes 6291460
  7.2 68.3 %all-gather.9.cloned.1.call-start = ((), (), s32[]{:S(2)}) async-start(), calls=%async_computation.2 | async-start | bytes 2949120 | tf_op jit(solution)/shard_map/all_gather | solution.py:234
  12.4 0.8 copy-start.3
  15.9 23.4 %copy-start.6 = (bf16[256,256]{1,0:T(8,128)(2,1)S(1)}, bf16[256,256]{1,0:T(8,128)(2,1)}, u32[]{:S(2)}) copy-start(bf16[256,256]{1,0:T(8,128)(2,1)} %param.27) | copy-start | bytes 393220
  15.9 23.4 %copy-start.12 = (f32[256]{0:T(256)S(1)}, f32[256]{0:T(256)}, u32[]{:S(2)}) copy-start(f32[256]{0:T(256)} %param.28) | copy-start | bytes 3076
  15.9 23.8 %copy-start.9 = (f32[4,256]{1,0:T(4,128)S(1)}, f32[4,256]{1,0:T(4,128)}, u32[]{:S(2)}) copy-start(f32[4,256]{1,0:T(4,128)} %param.29) | copy-start | bytes 12292
  15.9 23.9 %copy-start.7 = (bf16[256,256]{1,0:T(8,128)(2,1)S(1)}, bf16[256,256]{1,0:T(8,128)(2,1)}, u32[]{:S(2)}) copy-start(bf16[256,256]{1,0:T(8,128)(2,1)} %param.24) | copy-start | bytes 393220
  39.2 121.3 %all-gather.11.cloned.1.call-start = ((), (), s32[]{:S(2)}) async-start(), calls=%async_computation.3 | async-start | bytes 5898240 | tf_op jit(solution)/shard_map/all_gather | solution.py:250
  75.5 5.2 %copy-start.13 = (bf16[1,2048,1024]{2,1,0:T(8,128)(2,1)S(1)}, bf16[1,2048,1024]{2,1,0:T(8,128)(2,1)}, u32[]{:S(2)}) copy-start(bf16[1,2048,1024]{2,1,0:T(8,128)(2,1)} %param.37) | copy-start | bytes 12582916
  75.5 5.3 %copy-start.14 = (bf16[576,2048]{1,0:T(8,128)(2,1)S(1)}, bf16[576,2048]{1,0:T(8,128)(2,1)}, u32[]{:S(2)}) copy-start(bf16[576,2048]{1,0:T(8,128)(2,1)} %all-gather.9.cloned.1.call-done) | copy-start | bytes 7077892
  84.7 88.0 %all-gather.7.cloned.1.call-start = ((), (), s32[]{:S(2)}) async-start(), calls=%async_computation.1 | async-start | bytes 1310720 | tf_op jit(solution)/shard_map/all_gather | solution.py:246
  93.6 30.1 %copy-start.5 = (bf16[4,64,4,128]{3,2,1,0:T(4,128)(2,1)S(1)}, bf16[4,64,4,128]{3,2,1,0:T(4,128)(2,1)}, u32[]{:S(2)}) copy-start(bf16[4,64,4,128]{3,2,1,0:T(4,128)(2,1)} %reshape.248) | copy-start | bytes 786436
  123.7 9.3 %copy-start.2 = (f32[4,64,4,64]{3,2,1,0:T(4,128)S(1)}, f32[4,64,4,64]{3,2,1,0:T(4,128)}, u32[]{:S(2)}) copy-start(f32[4,64,4,64]{3,2,1,0:T(4,128)} %reshape.258) | copy-start | bytes 786436
  133.0 4.6 %copy-start.10 = (f32[512]{0:T(512)S(1)}, f32[512]{0:T(512)}, u32[]{:S(2)}) copy-start(f32[512]{0:T(512)} %param.30) | copy-start | bytes 6148
  135.8 3.7 %copy-start.8 = (s32[96,4]{0,1:T(4,128)S(1)}, s32[96,4]{0,1:T(4,128)}, u32[]{:S(2)}) copy-start(s32[96,4]{0,1:T(4,128)} %param.34) | copy-start | bytes 4612
  135.8 7.4 %copy-start.4 = (bf16[96,2048]{1,0:T(8,128)(2,1)S(1)}, bf16[96,2048]{1,0:T(8,128)(2,1)}, u32[]{:S(2)}) copy-start(bf16[96,2048]{1,0:T(8,128)(2,1)} %copy-done.3) | copy-start | bytes 1179652
  140.3 18.3 %copy-start.1 = (bf16[1024,512]{1,0:T(8,128)(2,1)S(1)}, bf16[1024,512]{1,0:T(8,128)(2,1)}, u32[]{:S(2)}) copy-start(bf16[1024,512]{1,0:T(8,128)(2,1)} %param.41) | copy-start | bytes 3145732
  157.6 2.1 %copy-start.11 = (pred[96,4]{0,1:T(4,128)(4,1)S(1)}, pred[96,4]{0,1:T(4,128)(4,1)}, u32[]{:S(2)}) copy-start(pred[96,4]{0,1:T(4,128)(4,1)} %compare_and_fusion) | copy-start | bytes 1156
  166.9 5.6 %collective-permute-start = (bf16[1,1,72,512]{3,2,0,1:T(8,128)(2,1)S(1)}, bf16[1,1,72,512]{3,2,0,1:T(8,128)(2,1)S(1)}, u32[]{:S(2)}, u32[]{:S(2)}) collective-permute-start(bf16[1,1,72,512]{3,2,0,1:T(8,128)(2,1)S(1)} %constant_dynamic-slice_fusion.6), channel_id=1, source_target_pairs={{0,4},{4,8},{8,12},{12,16},{16,20},{20,24},{24,28},{28,0},{1,5},{5... | collective-permute-start | bytes 221192 | tf_op jit(solution)/shard_map/ppermute | solution.py:31
  172.6 9.2 %collective-permute-start.1 = (bf16[1,1,72,512]{3,2,0,1:T(8,128)(2,1)S(1)}, bf16[1,1,72,512]{3,2,0,1:T(8,128)(2,1)S(1)}, u32[]{:S(2)}, u32[]{:S(2)}) collective-permute-start(bf16[1,1,72,512]{3,2,0,1:T(8,128)(2,1)S(1)} %get-tuple-element.192), channel_id=1, source_target_pairs={{0,8},{4,12},{8,16},{12,20},{16,24},{20,28},{24,0},{28,4},{1,9},{5... | collective-permute-start | bytes 221192 | tf_op jit(solution)/shard_map/ppermute | solution.py:31
  175.4 7.2 %collective-permute-start.2 = (bf16[1,1,72,512]{3,2,0,1:T(8,128)(2,1)S(1)}, bf16[1,1,72,512]{3,2,0,1:T(8,128)(2,1)S(1)}, u32[]{:S(2)}, u32[]{:S(2)}) collective-permute-start(bf16[1,1,72,512]{3,2,0,1:T(8,128)(2,1)S(1)} %get-tuple-element.191), channel_id=1, source_target_pairs={{0,12},{4,16},{8,20},{12,24},{16,28},{20,0},{24,4},{28,8},{1,13},{... | collective-permute-start | bytes 221192 | tf_op jit(solution)/shard_map/ppermute | solution.py:31
  175.4 8.9 %collective-permute-start.3 = (bf16[1,1,72,512]{3,2,0,1:T(8,128)(2,1)S(1)}, bf16[1,1,72,512]{3,2,0,1:T(8,128)(2,1)S(1)}, u32[]{:S(2)}, u32[]{:S(2)}) collective-permute-start(bf16[1,1,72,512]{3,2,0,1:T(8,128)(2,1)S(1)} %get-tuple-element.190), channel_id=1, source_target_pairs={{0,16},{4,20},{8,24},{12,28},{16,0},{20,4},{24,8},{28,12},{1,17},{... | collective-permute-start | bytes 221192 | tf_op jit(solution)/shard_map/ppermute | solution.py:31
  176.4 7.9 %collective-permute-start.4 = (bf16[1,1,72,512]{3,2,0,1:T(8,128)(2,1)S(1)}, bf16[1,1,72,512]{3,2,0,1:T(8,128)(2,1)S(1)}, u32[]{:S(2)}, u32[]{:S(2)}) collective-permute-start(bf16[1,1,72,512]{3,2,0,1:T(8,128)(2,1)S(1)} %get-tuple-element.189), channel_id=1, source_target_pairs={{0,20},{4,24},{8,28},{12,0},{16,4},{20,8},{24,12},{28,16},{1,21},{... | collective-permute-start | bytes 221192 | tf_op jit(solution)/shard_map/ppermute | solution.py:31
  178.0 7.0 %collective-permute-start.5 = (bf16[1,1,72,512]{3,2,0,1:T(8,128)(2,1)S(1)}, bf16[1,1,72,512]{3,2,0,1:T(8,128)(2,1)S(1)}, u32[]{:S(2)}, u32[]{:S(2)}) collective-permute-start(bf16[1,1,72,512]{3,2,0,1:T(8,128)(2,1)S(1)} %get-tuple-element.188), channel_id=1, source_target_pairs={{0,24},{4,28},{8,0},{12,4},{16,8},{20,12},{24,16},{28,20},{1,25},{... | collective-permute-start | bytes 221192 | tf_op jit(solution)/shard_map/ppermute | solution.py:31
  181.8 3.2 %collective-permute-start.6 = (bf16[1,1,72,512]{3,2,0,1:T(8,128)(2,1)S(1)}, bf16[1,1,72,512]{3,2,0,1:T(8,128)(2,1)S(1)}, u32[]{:S(2)}, u32[]{:S(2)}) collective-permute-start(bf16[1,1,72,512]{3,2,0,1:T(8,128)(2,1)S(1)} %get-tuple-element.187), channel_id=1, source_target_pairs={{0,28},{4,0},{8,4},{12,8},{16,12},{20,16},{24,20},{28,24},{1,29},{... | collective-permute-start | bytes 221192 | tf_op jit(solution)/shard_map/ppermute | solution.py:31
Sparse Core Ops, SparseCore 0:
  39.3 36.1 all-gather.8
  84.8 56.9 all-gather.10
  144.2 26.3 all-gather.6
